TPU v7x, 128 devices: a whole 4x4x4 slice. The times are simulated.
128 devices in a mesh: sp: 64 (over z, y, x), tp: 2 (over core).
Axes of the slice: x: 4, y: 4, z: 4, core: 2. Of those that a mesh axis runs over, the one named last changes fastest.
Arguments:
- features: bfloat16 [32768, 4096], P('sp', 'tp'), may hold values from -16 to 16
- weight_value: bfloat16 [4096, 1024], P(None, 'tp'), may hold values from -0.09375 to 0.09375
- weight_gate: bfloat16 [4096, 1024], P(None, 'tp'), may hold values from -0.09375 to 0.09375
- weight_out: bfloat16 [4096, 1024], P(None, 'tp'), may hold values from -0.1875 to 0.1875
- conv_taps: float32 [31, 1024], P(None, 'tp'), may hold values from -6 to 6
- norm_gain: float32 [1024], P('tp'), may hold values from 0.1 to 1.9
- out_grad: bfloat16 [32768, 4096], P('sp', 'tp'), may hold values from -16 to 16
Outputs:
- value_grad: float32 [32768, 1024], P('sp', 'tp')
- gate_grad: float32 [32768, 1024], P('sp', 'tp')
- value_wgrad: float32 [4096, 1024], P('sp', 'tp')
- gate_wgrad: float32 [4096, 1024], P('sp', 'tp')
- out_wgrad: float32 [4096, 1024], P('sp', 'tp')
- taps_grad: float32 [31, 1024], P(None, 'tp')
- gain_grad: float32 [1024], P('tp')
All inputs are finite; a program needn't handle non-finite values.
Results may differ from a plain program's by a relative error of at most 0.0057.
Values may be sent and summed in bfloat16 or wider, within the bound.
A program may use at most 192 MiB of HBM per device.

v0:
```python
import jax
import jax.numpy as jnp
from jax import lax
from jax.sharding import Mesh
from jax.sharding import PartitionSpec as P

SP = ("sp_0", "sp_1", "sp_2")
NORM_EPS = 1e-05


def sum_by_axis(running, axes):
    for axis in axes:
        running = lax.psum_scatter(running, axis, scatter_dimension=0, tiled=True)
    return running


def in_one_piece(arrays, axis, dim, along):
    ends, at = ([], 0)
    for a in arrays[:-1]:
        at += a.shape[along]
        ends.append(at)
    both = jnp.concatenate(arrays, axis=along)
    return tuple(jnp.split(lax.all_gather(both, axis, axis=dim, tiled=True), ends, axis=along))


def with_halo(block, sides, width):
    for axis, dim in sides:
        count = lax.axis_size(axis)
        forward = [(i, i + 1) for i in range(count - 1)]
        backward = [(target, source) for source, target in forward]
        low = lax.ppermute(
            lax.slice_in_dim(block, block.shape[dim] - width, None, axis=dim), axis, forward
        )
        high = lax.ppermute(lax.slice_in_dim(block, 0, width, axis=dim), axis, backward)
        block = jnp.concatenate([low, block, high], axis=dim)
    return block


def from_everyone(x, axis):
    devices = lax.axis_size(axis)
    return lax.all_to_all(jnp.broadcast_to(x[None], (devices, *x.shape)), axis, 0, 0, tiled=True)


def of_everyone(x, axis):
    return from_everyone(x, axis).sum(axis=0)


def packed_total(arrays, axis):
    vector, at, finished = (jnp.concatenate([a.reshape(-1) for a in arrays]), 0, [])
    running = of_everyone(vector, axis)
    for a in arrays:
        finished.append(running[at : at + a.size].reshape(a.shape))
        at += a.size
    return tuple(finished)


def total_of_pieces(x, axis):
    return lax.all_gather(x, axis).sum(0)


def make_term(left_rows, right_rows):
    return lax.dot_general(
        left_rows, right_rows, (((0,), (0,)), ((), ())), preferred_element_type=jnp.float32
    )


def out_weight_sum(whole_cotangent, act_half):
    term = make_term(whole_cotangent, act_half).astype(jnp.bfloat16)
    return sum_by_axis(term, SP).astype(jnp.float32)


def on_device(features, weight_value, weight_gate, weight_out, conv_taps, norm_gain, out_grad):
    whole_inputs, whole_cotangent = in_one_piece((features, out_grad), "tp", 1, 0)
    value_half = jnp.dot(whole_inputs, weight_value, preferred_element_type=jnp.float32).astype(
        jnp.bfloat16
    )
    gate_half = jnp.dot(whole_inputs, weight_gate, preferred_element_type=jnp.float32).astype(
        jnp.bfloat16
    )
    value_half, gate_half = lax.optimization_barrier((value_half, gate_half))
    value_pre = value_half.astype(jnp.float32)
    gate_pre = gate_half.astype(jnp.float32)
    gate_sig = jax.nn.sigmoid(gate_pre)
    mixed_half = lax.optimization_barrier((value_pre * gate_sig).astype(jnp.bfloat16))
    tap_count = conv_taps.shape[0]
    half_width = tap_count // 2
    row_count = mixed_half.shape[0]
    channels = mixed_half.shape[1] * lax.axis_size("tp")
    extended = with_halo(mixed_half, ((SP, 0),), half_width).astype(jnp.float32)
    conv_out = jnp.zeros(mixed_half.shape, jnp.float32)
    for offset in range(tap_count):
        conv_out = conv_out + conv_taps[offset] * extended[offset : offset + row_count]
    row_sum, row_square = packed_total(
        (jnp.sum(conv_out, axis=-1), jnp.sum(conv_out * conv_out, axis=-1)), "tp"
    )
    mean_row = row_sum[:, None] / channels
    var_row = row_square[:, None] / channels - mean_row * mean_row
    inv_std = lax.rsqrt(var_row + NORM_EPS)
    normed = (conv_out - mean_row) * inv_std
    pre_act = normed * norm_gain
    act_sig = jax.nn.sigmoid(pre_act)
    act_half = (pre_act * act_sig).astype(jnp.bfloat16)
    act_grad = jnp.dot(whole_cotangent, weight_out, preferred_element_type=jnp.float32)
    pre_grad = act_grad * act_sig * (1.0 + pre_act * (1.0 - act_sig))
    gain_part = jnp.sum(pre_grad * normed, axis=0)
    norm_grad = pre_grad * norm_gain
    first_sum, second_sum = packed_total(
        (jnp.sum(norm_grad, axis=-1), jnp.sum(norm_grad * normed, axis=-1)), "tp"
    )
    first_mom = first_sum[:, None] / channels
    second_mom = second_sum[:, None] / channels
    conv_grad = inv_std * (norm_grad - first_mom - normed * second_mom)
    grad_ext = with_halo(conv_grad, ((SP, 0),), half_width)
    mixed_grad = jnp.zeros(conv_grad.shape, jnp.float32)
    taps_rows = []
    for offset in range(tap_count):
        begin = 2 * half_width - offset
        mixed_grad = mixed_grad + conv_taps[offset] * grad_ext[begin : begin + row_count]
        taps_rows.append(jnp.sum(conv_grad * extended[offset : offset + row_count], axis=0))
    small = lax.psum(jnp.concatenate([jnp.stack(taps_rows), gain_part[None]], axis=0), SP)
    taps_grad, gain_grad = (small[:tap_count], small[tap_count])
    value_grad = mixed_grad * gate_sig
    gate_grad = mixed_grad * value_pre * gate_sig * (1.0 - gate_sig)
    value_low = value_grad.astype(jnp.bfloat16)
    gate_low = gate_grad.astype(jnp.bfloat16)
    out_wgrad = out_weight_sum(whole_cotangent, act_half)
    both_low = jnp.concatenate([value_low, gate_low], axis=1)
    joined = sum_by_axis(make_term(whole_inputs, both_low).astype(jnp.bfloat16), SP)
    joined = joined.astype(jnp.float32)
    split_at = value_low.shape[1]
    value_wgrad = joined[:, :split_at]
    gate_wgrad = joined[:, split_at:]
    return (value_grad, gate_grad, value_wgrad, gate_wgrad, out_wgrad, taps_grad, gain_grad)


def solution(mesh):
    split = Mesh(mesh.devices.reshape(4, 4, 4, mesh.shape["tp"]), ("sp_0", "sp_1", "sp_2", "tp"))
    return jax.shard_map(
        on_device,
        mesh=split,
        in_specs=(
            P(SP, "tp"),
            P(None, "tp"),
            P(None, "tp"),
            P(None, "tp"),
            P(None, "tp"),
            P("tp"),
            P(SP, "tp"),
        ),
        out_specs=(
            P(SP, "tp"),
            P(SP, "tp"),
            P(SP, "tp"),
            P(SP, "tp"),
            P(SP, "tp"),
            P(None, "tp"),
            P("tp"),
        ),
        check_vma=False,
    )
```

profile of v0, /device:TPU:0, one launch (start us, length us, event | category | flops | bytes accessed | tf_op | source)
XLA Modules:
  0.0 446.9 jit_solution(9746865256533950565)
XLA Ops:
  7.2 4.8 %pad_maximum_fusion = bf16[1024,2048]{1,0:T(8,128)(2,1)} fusion(bf16[512,2048]{1,0:T(8,128)(2,1)} %param.13, bf16[512,2048]{1,0:T(8,128)(2,1)} %param.7), kind=kLoop, calls=%fused_computation.30 | loop fusion | flops 8388608 | bytes 8388608 | tf_op jit(solution)/shard_map/concatenate | solution.py:22
  12.9 24.3 %all-gather.2.cloned.1.call-done = bf16[1024,4096]{1,0:T(8,128)(2,1)} async-done(((bf16[1024,2048]{1,0:T(8,128)(2,1)}), bf16[1024,4096]{1,0:T(8,128)(2,1)}) %all-gather.2.cloned.1.call-update) | async-done | bytes 8388624 | tf_op jit(solution)/shard_map/all_gather | solution.py:23
  37.2 5.9 %fusion.14 = bf16[512,512]{1,0:T(8,128)(2,1)S(1)} fusion(bf16[4096,512]{1,0:T(8,128)(2,1)} %param.8, bf16[1024,4096]{1,0:T(8,128)(2,1)} %all-gather.2.cloned.1.call-done), kind=kOutput, calls=%fused_computation.43 | convolution fusion | flops 2147745792 | bytes 8912896 | tf_op jit(solution)/shard_map/dot_general | solution.py:74
  44.2 2.3 fusion.17
  46.9 3.5 collective-permute-start
  50.4 1.3 collective-permute-start.1
  51.8 4.2 collective-permute-done.1
  56.2 5.1 %fusion.121 = (f32[512]{0:T(512)S(1)}, f32[512]{0:T(512)S(1)}, f32[512,512]{1,0:T(8,128)S(1)}) fusion(f32[542,512]{1,0:T(8,128)S(1)} %maximum_convert_fusion, f32[512]{0:T(512)S(1)} %bitcast.127, f32[512]{0:T(512)S(1)} %bitcast.129, f32[512]{0:T(512)S(1)} %bitcast.71, f32[512]{0:T(512)S(1)} %bitcast.73, f32[512]{0:T(512)S(1)} %bitcast.75, ...), kind=kLoop, calls=%fused_computation.219 | loop fusion | flops 16776192 | bytes 33622016 | tf_op jit(solution)/shard_map/reduce_sum | solution.py:94
  61.3 3.7 all_to_all.12
  65.0 6.7 %convolution_convert_fusion.1 = bf16[4096,512]{1,0:T(8,128)(2,1)} fusion(bf16[1024,4096]{1,0:T(8,128)(2,1)} %all-gather.2.cloned.1.call-done, f32[512,512]{1,0:T(8,128)S(1)} %get-tuple-element.53, f32[512]{0:T(512)S(1)} %copy-done.2, f32[512]{0:T(512)S(1)} %get-tuple-element.94, f32[512]{0:T(512)S(1)} %get-tuple-element.93), kind=kOutput, calls=%fused_computation.29 | convolution fusion | flops 2151677952 | bytes 9443328 | tf_op jit(solution)/shard_map/dot_general | solution.py:62
  71.8 7.1 %multiply_reduce_fusion = (f32[512]{0:T(512)S(1)}, f32[512]{0:T(512)S(1)}, f32[512]{0:T(512)S(1)}, f32[512,512]{1,0:T(8,128)}) fusion(f32[512,512]{1,0:T(8,128)S(1)} %get-tuple-element.53, f32[512]{0:T(512)S(1)} %get-tuple-element.94, f32[512]{0:T(512)S(1)} %get-tuple-element.93, f32[512]{0:T(512)S(1)} %copy-done.2, bf16[4096,512]{1,0:T(8,128)(2,1)} %param.10, ...), kind=kOutput, calls=%fused_computation.164 | convolution fusion | flops 2151938560 | bytes 10498048 | tf_op jit(solution)/shard_map/dot_general | solution.py:103
  79.0 3.7 all_to_all.13
  82.7 4.2 multiply_reduce_fusion.1
  86.9 1.3 collective-permute-start.2
  88.2 4.5 %collective-permute-start.3 = (f32[15,512]{1,0:T(8,128)S(1)}, f32[15,512]{1,0:T(8,128)S(1)}, u32[]{:S(2)}, u32[]{:S(2)}) collective-permute-start(f32[15,512]{1,0:T(8,128)S(1)} %get-tuple-element.55), channel_id=1, source_target_pairs={{0,2},{2,4},{4,6},{6,8},{8,10},{10,12},{12,14},{14,16},{16,18},{18... | collective-permute-start | bytes 92168 | tf_op jit(solution)/shard_map/ppermute | solution.py:31
  92.8 1.6 collective-permute-done.3
  94.4 5.9 %fusion.122 = (bf16[512,512]{1,0:T(8,128)(2,1)}, f32[512,512]{1,0:T(8,128)}, f32[512,512]{1,0:T(8,128)}) fusion(bf16[512,512]{1,0:T(8,128)(2,1)S(1)} %fusion.17, f32[512,512]{1,0:T(8,128)S(1)} %get-tuple-element.47, f32[15,512]{1,0:T(8,128)S(1)} %collective-permute-done.3, f32[512]{0:T(512)S(1)} %bitcast.128, f32[512]{0:T(512)S(1)} %bitcast.130, ...), kind=kLoop, calls=%fused_computation.220 | loop fusion | flops 25427968 | bytes 4319232 | tf_op jit(solution)/shard_map/convert_element_type | solution.py:124
  100.2 2.6 fusion.125
  102.8 10.2 %convolution_convert_fusion = bf16[4096,1024]{1,0:T(8,128)(2,1)} fusion(bf16[1024,4096]{1,0:T(8,128)(2,1)} %all-gather.2.cloned.1.call-done, bf16[512,512]{1,0:T(8,128)(2,1)S(1)} %get-tuple-element.51, bf16[512,512]{1,0:T(8,128)(2,1)} %get-tuple-element.48), kind=kOutput, calls=%fused_computation | convolution fusion | flops 4301258752 | bytes 13631488 | tf_op jit(solution)/shard_map/dot_general | solution.py:62
  113.0 10.5 %reduce-scatter.13.cloned.1.call-done = bf16[1024,512]{1,0:T(8,128)(2,1)} async-done(((bf16[4096,512]{1,0:T(8,128)(2,1)}), bf16[1024,512]{1,0:T(8,128)(2,1)}) %reduce-scatter.13.cloned.1.call-update) | async-done | bytes 1048592 | tf_op jit(solution)/shard_map/reduce_scatter | solution.py:13
  123.7 82.9 %reduce-scatter.7.cloned.1.call-done = bf16[1024,1024]{1,0:T(8,128)(2,1)} async-done(((bf16[4096,1024]{1,0:T(8,128)(2,1)}), bf16[1024,1024]{1,0:T(8,128)(2,1)}) %reduce-scatter.7.cloned.1.call-update) | async-done | bytes 2097168 | tf_op jit(solution)/shard_map/reduce_scatter | solution.py:13
  206.7 1.7 multiply_reduce_fusion.2
  208.4 2.5 concatenate.60
  211.0 21.2 %reduce-scatter.15.cloned.1.call-done = bf16[256,512]{1,0:T(8,128)(2,1)} async-done(((bf16[1024,512]{1,0:T(8,128)(2,1)}), bf16[256,512]{1,0:T(8,128)(2,1)}) %reduce-scatter.15.cloned.1.call-update) | async-done | bytes 262160 | tf_op jit(solution)/shard_map/reduce_scatter | solution.py:13
  232.3 31.7 %reduce-scatter.9.cloned.1.call-done = bf16[256,1024]{1,0:T(8,128)(2,1)} async-done(((bf16[1024,1024]{1,0:T(8,128)(2,1)}), bf16[256,1024]{1,0:T(8,128)(2,1)}) %reduce-scatter.9.cloned.1.call-update) | async-done | bytes 524304 | tf_op jit(solution)/shard_map/reduce_scatter | solution.py:13
  264.0 128.1 %all-reduce.2.cloned.1.call-done = f32[32,512]{1,0:T(8,128)} async-done(((f32[32,512]{1,0:T(8,128)}), f32[32,512]{1,0:T(8,128)}) %all-reduce.2.cloned.1.call-update) | async-done | bytes 65552 | tf_op jit(solution)/shard_map/psum | solution.py:120
  392.1 1.3 slice.602
  393.4 19.8 %reduce-scatter.17.cloned.1.call-done = bf16[64,512]{1,0:T(8,128)(2,1)} async-done(((bf16[256,512]{1,0:T(8,128)(2,1)}), bf16[64,512]{1,0:T(8,128)(2,1)}) %reduce-scatter.17.cloned.1.call-update) | async-done | bytes 65552 | tf_op jit(solution)/shard_map/reduce_scatter | solution.py:13
  413.2 1.5 convert_element_type.51
  414.7 22.3 %reduce-scatter.11.cloned.1.call-done = bf16[64,1024]{1,0:T(8,128)(2,1)} async-done(((bf16[256,1024]{1,0:T(8,128)(2,1)}), bf16[64,1024]{1,0:T(8,128)(2,1)}) %reduce-scatter.11.cloned.1.call-update) | async-done | bytes 131088 | tf_op jit(solution)/shard_map/reduce_scatter | solution.py:13
  437.0 1.6 fusion.129
  438.6 1.5 copy.23
  (42 shorter events, 3.0 us)
Async XLA Ops:
  7.2 30.0 %all-gather.2.cloned.1.call-start = ((), (), s32[]{:S(2)}) async-start(), calls=%async_computation.8 | async-start | bytes 12582912 | tf_op jit(solution)/shard_map/all_gather | solution.py:23
  12.0 0.8 copy-start.1
  12.0 111.6 %reduce-scatter.13.cloned.1.call-start = ((), (), s32[]{:S(2)}) async-start(), calls=%async_computation.12 | async-start | bytes 5242880 | tf_op jit(solution)/shard_map/reduce_scatter | solution.py:13
  37.2 5.9 %copy-start.3 = (bf16[1024,4096]{1,0:T(8,128)(2,1)S(1)}, bf16[1024,4096]{1,0:T(8,128)(2,1)}, u32[]{:S(2)}) copy-start(bf16[1024,4096]{1,0:T(8,128)(2,1)} %all-gather.2.cloned.1.call-done) | copy-start | bytes 25165828
  37.2 7.0 %copy-start.4 = (bf16[4096,512]{1,0:T(8,128)(2,1)S(1)}, bf16[4096,512]{1,0:T(8,128)(2,1)}, u32[]{:S(2)}) copy-start(bf16[4096,512]{1,0:T(8,128)(2,1)} %param.9) | copy-start | bytes 12582916
  46.9 4.9 %collective-permute-start = (bf16[15,512]{1,0:T(8,128)(2,1)S(1)}, bf16[15,512]{1,0:T(8,128)(2,1)S(1)}, u32[]{:S(2)}, u32[]{:S(2)}) collective-permute-start(bf16[15,512]{1,0:T(8,128)(2,1)S(1)} %get-tuple-element.56), channel_id=1, source_target_pairs={{0,2},{2,4},{4,6},{6,8},{8,10},{10,12},{12,14},{14,16},{16,18},{18... | collective-permute-start | bytes 46088 | tf_op jit(solution)/shard_map/ppermute | solution.py:31
  50.4 5.6 %collective-permute-start.1 = (bf16[15,512]{1,0:T(8,128)(2,1)S(1)}, bf16[15,512]{1,0:T(8,128)(2,1)S(1)}, u32[]{:S(2)}, u32[]{:S(2)}) collective-permute-start(bf16[15,512]{1,0:T(8,128)(2,1)S(1)} %get-tuple-element.57), channel_id=1, source_target_pairs={{2,0},{4,2},{6,4},{8,6},{10,8},{12,10},{14,12},{16,14},{18,16},{20... | collective-permute-start | bytes 46088 | tf_op jit(solution)/shard_map/ppermute | solution.py:34
  56.2 8.9 %copy-start.2 = (f32[512]{0:T(512)S(1)}, f32[512]{0:T(512)}, u32[]{:S(2)}) copy-start(f32[512]{0:T(512)} %param.12) | copy-start | bytes 6148
  61.2 10.6 %copy-start = (f32[512,512]{1,0:T(8,128)}, f32[512,512]{1,0:T(8,128)S(1)}, u32[]{:S(2)}) copy-start(f32[512,512]{1,0:T(8,128)S(1)} %get-tuple-element.53) | copy-start | bytes 3145732
  71.8 134.8 %reduce-scatter.7.cloned.1.call-start = ((), (), s32[]{:S(2)}) async-start(), calls=%async_computation.9 | async-start | bytes 10485760 | tf_op jit(solution)/shard_map/reduce_scatter | solution.py:13
  86.9 5.9 %collective-permute-start.2 = (f32[15,512]{1,0:T(8,128)S(1)}, f32[15,512]{1,0:T(8,128)S(1)}, u32[]{:S(2)}, u32[]{:S(2)}) collective-permute-start(f32[15,512]{1,0:T(8,128)S(1)} %get-tuple-element.54), channel_id=1, source_target_pairs={{2,0},{4,2},{6,4},{8,6},{10,8},{12,10},{14,12},{16,14},{18,16},{20... | collective-permute-start | bytes 92168 | tf_op jit(solution)/shard_map/ppermute | solution.py:34
  88.2 6.1 %collective-permute-start.3 = (f32[15,512]{1,0:T(8,128)S(1)}, f32[15,512]{1,0:T(8,128)S(1)}, u32[]{:S(2)}, u32[]{:S(2)}) collective-permute-start(f32[15,512]{1,0:T(8,128)S(1)} %get-tuple-element.55), channel_id=1, source_target_pairs={{0,2},{2,4},{4,6},{6,8},{8,10},{10,12},{12,14},{14,16},{16,18},{18... | collective-permute-start | bytes 92168 | tf_op jit(solution)/shard_map/ppermute | solution.py:31
  113.0 119.2 %reduce-scatter.15.cloned.1.call-start = ((), (), s32[]{:S(2)}) async-start(), calls=%async_computation.13 | async-start | bytes 1310720 | tf_op jit(solution)/shard_map/reduce_scatter | solution.py:13
  123.6 140.4 %reduce-scatter.9.cloned.1.call-start = ((), (), s32[]{:S(2)}) async-start(), calls=%async_computation.10 | async-start | bytes 2621440 | tf_op jit(solution)/shard_map/reduce_scatter | solution.py:13
  206.6 185.5 %all-reduce.2.cloned.1.call-start = ((), (), s32[]{:S(2)}) async-start(), calls=%async_computation.15 | async-start | bytes 131072 | tf_op jit(solution)/shard_map/psum | solution.py:120
  210.9 202.3 %reduce-scatter.17.cloned.1.call-start = ((), (), s32[]{:S(2)}) async-start(), calls=%async_computation.14 | async-start | bytes 327680 | tf_op jit(solution)/shard_map/reduce_scatter | solution.py:13
  232.2 204.7 %reduce-scatter.11.cloned.1.call-start = ((), (), s32[]{:S(2)}) async-start(), calls=%async_computation.11 | async-start | bytes 655360 | tf_op jit(solution)/shard_map/reduce_scatter | solution.py:13
Sparse Core Ops, SparseCore 0:
  12.1 25.0 all-gather.1
  71.9 51.6 reduce-scatter.12
  126.1 80.4 reduce-scatter.6
  208.8 23.3 reduce-scatter.14
  234.5 29.4 reduce-scatter.8
  269.1 123.0 all-reduce.1
  394.5 18.6 reduce-scatter.16
  415.6 21.3 reduce-scatter.10
where the time goes:
time: 448 us; the launch traced here: 447 us
  waiting for transfers between devices  347 us (77%)
  matrix products  32.2 us (7%)
  other arithmetic  26.2 us (6%)
  between operations  14.3 us (3%)
  starting transfers between devices  10.9 us (2%)
  local copies, waits for them, and re-layouts  8.86 us (2%)
  blocking collectives  7.42 us (2%)
    reduce_scatter x6, waiting for transfers between devices, sum_by_axis(): running = lax.psum_scatter(running, axis, scatter_dimension=0, tiled=True)  188 us
    psum x1, waiting for transfers between devices, on_device(): lax.psum(jnp.concatenate([jnp.stack(taps_rows), gain_part[None]], axis=0)...  128 us
    all_gather x1, waiting for transfers between devices, in_one_piece(): lax.all_gather(both, axis, axis=dim, tiled=True)  24.3 us
    dot_general x2, matrix products, make_term(): lax.dot_general(left_rows, right_rows, (((0,), (0,)), ((), ())), preferre...  16.9 us
  transfers between devices with their start and end apart: 12, of which 11 were waited for; matrix products, arithmetic and copies ran while one was open for 8% of the time, Pallas kernels for 0%

commit v1 on v0

--- a/solution.py
+++ b/solution.py
@@ -117,7 +117,9 @@
         begin = 2 * half_width - offset
         mixed_grad = mixed_grad + conv_taps[offset] * grad_ext[begin : begin + row_count]
         taps_rows.append(jnp.sum(conv_grad * extended[offset : offset + row_count], axis=0))
-    small = lax.psum(jnp.concatenate([jnp.stack(taps_rows), gain_part[None]], axis=0), SP)
+    small = jnp.sum(
+        lax.all_gather(jnp.concatenate([jnp.stack(taps_rows), gain_part[None]], axis=0), SP), axis=0
+    )
     taps_grad, gain_grad = (small[:tap_count], small[tap_count])
     value_grad = mixed_grad * gate_sig
     gate_grad = mixed_grad * value_pre * gate_sig * (1.0 - gate_sig)

time: 448 us -> 389 us (0.87)
  waiting for transfers between devices: 347 us -> 288 us
    psum x1 -> x0, waiting for transfers between devices: 128 us -> none  [on_device(): lax.psum(jnp.concatenate([jnp.stack(taps_rows), gain_part[None]], axis=0)...]
    all_gather x0 -> x1, waiting for transfers between devices: none -> 71.6 us  [on_device(): lax.all_gather(jnp.concatenate([jnp.stack(taps_rows), gain_part[None]], a...]
  transfers between devices with their start and end apart: 12 -> 12, of which waited for: 11 -> 11; matrix products, arithmetic and copies ran while one was open for 8% -> 10% of each run, Pallas kernels for 0% -> 0%
where the time goes in v1:
time: 389 us; the launch traced here: 388 us
  waiting for transfers between devices  288 us (74%)
  matrix products  32.2 us (8%)
  other arithmetic  28.7 us (7%)
  between operations  14.4 us (4%)
  starting transfers between devices  10.9 us (3%)
  blocking collectives  7.42 us (2%)
  local copies, waits for them, and re-layouts  6.68 us (2%)
    reduce_scatter x6, waiting for transfers between devices, sum_by_axis(): running = lax.psum_scatter(running, axis, scatter_dimension=0, tiled=True)  186 us
    all_gather x1, waiting for transfers between devices, on_device(): lax.all_gather(jnp.concatenate([jnp.stack(taps_rows), gain_part[None]], a...  71.6 us
    all_gather x1, waiting for transfers between devices, in_one_piece(): lax.all_gather(both, axis, axis=dim, tiled=True)  24.3 us
    dot_general x2, matrix products, make_term(): lax.dot_general(left_rows, right_rows, (((0,), (0,)), ((), ())), preferre...  16.9 us
    ppermute x2, starting transfers between devices, with_halo(): lax.ppermute(lax.slice_in_dim(block, block.shape[dim] - width, None, axis...  8.03 us
  transfers between devices with their start and end apart: 12, of which 11 were waited for; matrix products, arithmetic and copies ran while one was open for 10% of the time, Pallas kernels for 0%

profile of v1, /device:TPU:0, one launch (start us, length us, event | category | flops | bytes accessed | tf_op | source)
XLA Modules:
  0.0 388.4 jit_solution(4725386152980991302)
XLA Ops:
  7.2 4.8 %pad_maximum_fusion = bf16[1024,2048]{1,0:T(8,128)(2,1)} fusion(bf16[512,2048]{1,0:T(8,128)(2,1)} %param.13, bf16[512,2048]{1,0:T(8,128)(2,1)} %param.7), kind=kLoop, calls=%fused_computation.30 | loop fusion | flops 8388608 | bytes 8388608 | tf_op jit(solution)/shard_map/concatenate | solution.py:22
  12.9 24.3 %all-gather.4.cloned.1.call-done = bf16[1024,4096]{1,0:T(8,128)(2,1)} async-done(((bf16[1024,2048]{1,0:T(8,128)(2,1)}), bf16[1024,4096]{1,0:T(8,128)(2,1)}) %all-gather.4.cloned.1.call-update) | async-done | bytes 8388624 | tf_op jit(solution)/shard_map/all_gather | solution.py:23
  37.2 5.9 %fusion.14 = bf16[512,512]{1,0:T(8,128)(2,1)S(1)} fusion(bf16[4096,512]{1,0:T(8,128)(2,1)} %param.8, bf16[1024,4096]{1,0:T(8,128)(2,1)} %all-gather.4.cloned.1.call-done), kind=kOutput, calls=%fused_computation.43 | convolution fusion | flops 2147745792 | bytes 8912896 | tf_op jit(solution)/shard_map/dot_general | solution.py:74
  43.1 1.1 copy-done.5
  44.2 2.3 fusion.17
  46.9 3.5 collective-permute-start
  50.4 1.3 collective-permute-start.1
  51.8 4.2 %collective-permute-done.1 = bf16[15,512]{1,0:T(8,128)(2,1)S(1)} collective-permute-done((bf16[15,512]{1,0:T(8,128)(2,1)S(1)}, bf16[15,512]{1,0:T(8,128)(2,1)S(1)}, u32[]{:S(2)}, u32[]{:S(2)}) %collective-permute-start.1) | collective-permute-done | bytes 15392 | tf_op jit(solution)/shard_map/ppermute | solution.py:34
  56.2 5.1 %fusion.121 = (f32[512]{0:T(512)S(1)}, f32[512]{0:T(512)S(1)}, f32[512,512]{1,0:T(8,128)S(1)}) fusion(f32[542,512]{1,0:T(8,128)S(1)} %maximum_convert_fusion, f32[512]{0:T(512)S(1)} %bitcast.129, f32[512]{0:T(512)S(1)} %bitcast.131, f32[512]{0:T(512)S(1)} %bitcast.73, f32[512]{0:T(512)S(1)} %bitcast.75, f32[512]{0:T(512)S(1)} %bitcast.77, ...), kind=kLoop, calls=%fused_computation.219 | loop fusion | flops 16776192 | bytes 33622016 | tf_op jit(solution)/shard_map/reduce_sum | solution.py:94
  61.3 3.7 all_to_all.12
  65.0 6.7 %convolution_convert_fusion.1 = bf16[4096,512]{1,0:T(8,128)(2,1)} fusion(bf16[1024,4096]{1,0:T(8,128)(2,1)} %all-gather.4.cloned.1.call-done, f32[512,512]{1,0:T(8,128)S(1)} %get-tuple-element.53, f32[512]{0:T(512)S(1)} %copy-done.3, f32[512]{0:T(512)S(1)} %get-tuple-element.94, f32[512]{0:T(512)S(1)} %get-tuple-element.93), kind=kOutput, calls=%fused_computation.29 | convolution fusion | flops 2151677952 | bytes 9443328 | tf_op jit(solution)/shard_map/dot_general | solution.py:62
  71.8 7.1 %multiply_reduce_fusion = (f32[512]{0:T(512)S(1)}, f32[512]{0:T(512)S(1)}, f32[512]{0:T(512)S(1)}, f32[512,512]{1,0:T(8,128)}) fusion(f32[512,512]{1,0:T(8,128)S(1)} %get-tuple-element.53, f32[512]{0:T(512)S(1)} %get-tuple-element.94, f32[512]{0:T(512)S(1)} %get-tuple-element.93, f32[512]{0:T(512)S(1)} %copy-done.3, bf16[4096,512]{1,0:T(8,128)(2,1)} %param.10, ...), kind=kOutput, calls=%fused_computation.164 | convolution fusion | flops 2151938560 | bytes 10498048 | tf_op jit(solution)/shard_map/dot_general | solution.py:103
  79.0 3.7 all_to_all.13
  82.7 4.2 %multiply_reduce_fusion.1 = (f32[512]{0:T(512)S(1)}, f32[512]{0:T(512)S(1)}, f32[512]{0:T(512)S(1)}, f32[512]{0:T(512)S(1)}, f32[512]{0:T(512)S(1)}, /*index=5*/...) fusion(f32[542,512]{1,0:T(8,128)S(1)} %maximum_convert_fusion, ...), kind=kLoop, calls=%fused_computation.165 | loop fusion | flops 11262976 | bytes 22067200 | tf_op jit(solution)/shard_map/reduce_sum | solution.py:119
  86.9 1.3 collective-permute-start.2
  88.2 4.5 %collective-permute-start.3 = (f32[15,512]{1,0:T(8,128)S(1)}, f32[15,512]{1,0:T(8,128)S(1)}, u32[]{:S(2)}, u32[]{:S(2)}) collective-permute-start(f32[15,512]{1,0:T(8,128)S(1)} %get-tuple-element.55), channel_id=1, source_target_pairs={{0,2},{2,4},{4,6},{6,8},{8,10},{10,12},{12,14},{14,16},{16,18},{18... | collective-permute-start | bytes 92168 | tf_op jit(solution)/shard_map/ppermute | solution.py:31
  92.8 1.6 collective-permute-done.3
  94.4 5.9 %fusion.122 = (bf16[512,512]{1,0:T(8,128)(2,1)}, f32[512,512]{1,0:T(8,128)}, f32[512,512]{1,0:T(8,128)}) fusion(bf16[512,512]{1,0:T(8,128)(2,1)S(1)} %fusion.17, f32[512,512]{1,0:T(8,128)S(1)} %get-tuple-element.47, f32[15,512]{1,0:T(8,128)S(1)} %collective-permute-done.3, f32[512]{0:T(512)S(1)} %bitcast.130, f32[512]{0:T(512)S(1)} %bitcast.132, ...), kind=kLoop, calls=%fused_computation.220 | loop fusion | flops 25427968 | bytes 4319232 | tf_op jit(solution)/shard_map/convert_element_type | solution.py:126
  100.2 2.6 fusion.125
  102.8 10.2 %convolution_convert_fusion = bf16[4096,1024]{1,0:T(8,128)(2,1)} fusion(bf16[1024,4096]{1,0:T(8,128)(2,1)} %all-gather.4.cloned.1.call-done, bf16[512,512]{1,0:T(8,128)(2,1)S(1)} %get-tuple-element.51, bf16[512,512]{1,0:T(8,128)(2,1)} %get-tuple-element.48), kind=kOutput, calls=%fused_computation | convolution fusion | flops 4301258752 | bytes 13631488 | tf_op jit(solution)/shard_map/dot_general | solution.py:62
  113.0 10.5 %reduce-scatter.13.cloned.1.call-done = bf16[1024,512]{1,0:T(8,128)(2,1)} async-done(((bf16[4096,512]{1,0:T(8,128)(2,1)}), bf16[1024,512]{1,0:T(8,128)(2,1)}) %reduce-scatter.13.cloned.1.call-update) | async-done | bytes 1048592 | tf_op jit(solution)/shard_map/reduce_scatter | solution.py:13
  123.7 82.9 %reduce-scatter.7.cloned.1.call-done = bf16[1024,1024]{1,0:T(8,128)(2,1)} async-done(((bf16[4096,1024]{1,0:T(8,128)(2,1)}), bf16[1024,1024]{1,0:T(8,128)(2,1)}) %reduce-scatter.7.cloned.1.call-update) | async-done | bytes 2097168 | tf_op jit(solution)/shard_map/reduce_scatter | solution.py:13
  206.7 1.7 multiply_reduce_fusion.2
  208.4 2.5 concatenate.60
  211.0 21.2 %reduce-scatter.15.cloned.1.call-done = bf16[256,512]{1,0:T(8,128)(2,1)} async-done(((bf16[1024,512]{1,0:T(8,128)(2,1)}), bf16[256,512]{1,0:T(8,128)(2,1)}) %reduce-scatter.15.cloned.1.call-update) | async-done | bytes 262160 | tf_op jit(solution)/shard_map/reduce_scatter | solution.py:13
  232.3 31.7 %reduce-scatter.9.cloned.1.call-done = bf16[256,1024]{1,0:T(8,128)(2,1)} async-done(((bf16[1024,1024]{1,0:T(8,128)(2,1)}), bf16[256,1024]{1,0:T(8,128)(2,1)}) %reduce-scatter.9.cloned.1.call-update) | async-done | bytes 524304 | tf_op jit(solution)/shard_map/reduce_scatter | solution.py:13
  264.0 71.6 %all-gather.6.cloned.1.call-done = f32[2048,512]{1,0:T(8,128)} async-done(((f32[32,512]{1,0:T(8,128)}), f32[2048,512]{1,0:T(8,128)}) %all-gather.6.cloned.1.call-update) | async-done | bytes 4194320 | tf_op jit(solution)/shard_map/all_gather | solution.py:121
  335.6 2.5 reduce_sum.389
  338.7 17.5 %reduce-scatter.17.cloned.1.call-done = bf16[64,512]{1,0:T(8,128)(2,1)} async-done(((bf16[256,512]{1,0:T(8,128)(2,1)}), bf16[64,512]{1,0:T(8,128)(2,1)}) %reduce-scatter.17.cloned.1.call-update) | async-done | bytes 65552 | tf_op jit(solution)/shard_map/reduce_scatter | solution.py:13
  356.2 1.5 convert_element_type.51
  357.7 22.3 %reduce-scatter.11.cloned.1.call-done = bf16[64,1024]{1,0:T(8,128)(2,1)} async-done(((bf16[256,1024]{1,0:T(8,128)(2,1)}), bf16[64,1024]{1,0:T(8,128)(2,1)}) %reduce-scatter.11.cloned.1.call-update) | async-done | bytes 131088 | tf_op jit(solution)/shard_map/reduce_scatter | solution.py:13
  379.9 1.6 fusion.129
  (44 shorter events, 2.5 us)
Async XLA Ops:
  7.2 30.0 %all-gather.4.cloned.1.call-start = ((), (), s32[]{:S(2)}) async-start(), calls=%async_computation.8 | async-start | bytes 12582912 | tf_op jit(solution)/shard_map/all_gather | solution.py:23
  12.0 0.8 copy-start.2
  12.0 111.6 %reduce-scatter.13.cloned.1.call-start = ((), (), s32[]{:S(2)}) async-start(), calls=%async_computation.12 | async-start | bytes 5242880 | tf_op jit(solution)/shard_map/reduce_scatter | solution.py:13
  37.2 5.9 %copy-start.4 = (bf16[1024,4096]{1,0:T(8,128)(2,1)S(1)}, bf16[1024,4096]{1,0:T(8,128)(2,1)}, u32[]{:S(2)}) copy-start(bf16[1024,4096]{1,0:T(8,128)(2,1)} %all-gather.4.cloned.1.call-done) | copy-start | bytes 25165828
  37.2 7.0 %copy-start.5 = (bf16[4096,512]{1,0:T(8,128)(2,1)S(1)}, bf16[4096,512]{1,0:T(8,128)(2,1)}, u32[]{:S(2)}) copy-start(bf16[4096,512]{1,0:T(8,128)(2,1)} %param.9) | copy-start | bytes 12582916
  46.9 4.9 %collective-permute-start = (bf16[15,512]{1,0:T(8,128)(2,1)S(1)}, bf16[15,512]{1,0:T(8,128)(2,1)S(1)}, u32[]{:S(2)}, u32[]{:S(2)}) collective-permute-start(bf16[15,512]{1,0:T(8,128)(2,1)S(1)} %get-tuple-element.56), channel_id=1, source_target_pairs={{0,2},{2,4},{4,6},{6,8},{8,10},{10,12},{12,14},{14,16},{16,18},{18... | collective-permute-start | bytes 46088 | tf_op jit(solution)/shard_map/ppermute | solution.py:31
  50.4 5.6 %collective-permute-start.1 = (bf16[15,512]{1,0:T(8,128)(2,1)S(1)}, bf16[15,512]{1,0:T(8,128)(2,1)S(1)}, u32[]{:S(2)}, u32[]{:S(2)}) collective-permute-start(bf16[15,512]{1,0:T(8,128)(2,1)S(1)} %get-tuple-element.57), channel_id=1, source_target_pairs={{2,0},{4,2},{6,4},{8,6},{10,8},{12,10},{14,12},{16,14},{18,16},{20... | collective-permute-start | bytes 46088 | tf_op jit(solution)/shard_map/ppermute | solution.py:34
  56.2 8.9 %copy-start.3 = (f32[512]{0:T(512)S(1)}, f32[512]{0:T(512)}, u32[]{:S(2)}) copy-start(f32[512]{0:T(512)} %param.12) | copy-start | bytes 6148
  61.2 10.6 %copy-start = (f32[512,512]{1,0:T(8,128)}, f32[512,512]{1,0:T(8,128)S(1)}, u32[]{:S(2)}) copy-start(f32[512,512]{1,0:T(8,128)S(1)} %get-tuple-element.53) | copy-start | bytes 3145732
  71.8 134.8 %reduce-scatter.7.cloned.1.call-start = ((), (), s32[]{:S(2)}) async-start(), calls=%async_computation.9 | async-start | bytes 10485760 | tf_op jit(solution)/shard_map/reduce_scatter | solution.py:13
  86.9 5.9 %collective-permute-start.2 = (f32[15,512]{1,0:T(8,128)S(1)}, f32[15,512]{1,0:T(8,128)S(1)}, u32[]{:S(2)}, u32[]{:S(2)}) collective-permute-start(f32[15,512]{1,0:T(8,128)S(1)} %get-tuple-element.54), channel_id=1, source_target_pairs={{2,0},{4,2},{6,4},{8,6},{10,8},{12,10},{14,12},{16,14},{18,16},{20... | collective-permute-start | bytes 92168 | tf_op jit(solution)/shard_map/ppermute | solution.py:34
  88.2 6.1 %collective-permute-start.3 = (f32[15,512]{1,0:T(8,128)S(1)}, f32[15,512]{1,0:T(8,128)S(1)}, u32[]{:S(2)}, u32[]{:S(2)}) collective-permute-start(f32[15,512]{1,0:T(8,128)S(1)} %get-tuple-element.55), channel_id=1, source_target_pairs={{0,2},{2,4},{4,6},{6,8},{8,10},{10,12},{12,14},{14,16},{16,18},{18... | collective-permute-start | bytes 92168 | tf_op jit(solution)/shard_map/ppermute | solution.py:31
  113.0 119.2 %reduce-scatter.15.cloned.1.call-start = ((), (), s32[]{:S(2)}) async-start(), calls=%async_computation.13 | async-start | bytes 1310720 | tf_op jit(solution)/shard_map/reduce_scatter | solution.py:13
  123.6 140.4 %reduce-scatter.9.cloned.1.call-start = ((), (), s32[]{:S(2)}) async-start(), calls=%async_computation.10 | async-start | bytes 2621440 | tf_op jit(solution)/shard_map/reduce_scatter | solution.py:13
  206.6 129.0 %all-gather.6.cloned.1.call-start = ((), (), s32[]{:S(2)}) async-start(), calls=%async_computation.15 | async-start | bytes 4259840 | tf_op jit(solution)/shard_map/all_gather | solution.py:121
  210.9 145.2 %reduce-scatter.17.cloned.1.call-start = ((), (), s32[]{:S(2)}) async-start(), calls=%async_computation.14 | async-start | bytes 327680 | tf_op jit(solution)/shard_map/reduce_scatter | solution.py:13
  232.2 147.7 %reduce-scatter.11.cloned.1.call-start = ((), (), s32[]{:S(2)}) async-start(), calls=%async_computation.11 | async-start | bytes 655360 | tf_op jit(solution)/shard_map/reduce_scatter | solution.py:13
  338.1 43.4 %copy-start.1 = (f32[32,512]{1,0:T(8,128)}, f32[32,512]{1,0:T(8,128)S(1)}, u32[]{:S(2)}) copy-start(f32[32,512]{1,0:T(8,128)S(1)} %reduce_sum.389) | copy-start | bytes 196612
Sparse Core Ops, SparseCore 0:
  12.1 25.0 all-gather.3
  71.9 51.6 reduce-scatter.12
  126.1 80.4 reduce-scatter.6
  208.8 23.3 reduce-scatter.14
  234.5 29.4 reduce-scatter.8
  267.3 68.2 all-gather.5
  338.0 18.1 reduce-scatter.16
  358.5 21.3 reduce-scatter.10
